TPU v7x, 32 devices: a whole 2x2x4 slice. The times are simulated.
32 devices in a mesh: sp: 8 (over z, y), dp: 4 (over x, core).
Axes of the slice: x: 2, y: 2, z: 4, core: 2. Of those that a mesh axis runs over, the one named last changes fastest.
Arguments:
- skip_connection_stream: bfloat16 [4, 1024, 2048], P('dp', 'sp'), may hold values from -6 to 6
- emitted_valve_unscaled: bfloat16 [4, 1024, 1024], P('dp', 'sp'), may hold values from -6 to 6
- channel_source_mapped: bfloat16 [4, 1024, 1024], P('dp', 'sp'), may hold values from -6 to 6
- hidden_source_mapped: bfloat16 [4, 1024, 256], P('dp', 'sp'), may hold values from -6 to 6
- probe_mapped_values: bfloat16 [4, 1024, 256], P('dp', 'sp'), may hold values from -6 to 6
- increment_premapped: float32 [4, 1024, 16], P('dp', None, 'sp'), may hold values from -6 to 6
- extra_log_fading: float32 [4, 1024, 16], P('dp', None, 'sp'), may hold values from -2 to 0
- channel_fading_speed: float32 [16], replicated, may hold values from 0 to 1, as said below
- channel_source_kernel: float32 [4, 1024], replicated, may hold values from -3 to 3
- hidden_source_kernel: float32 [4, 256], replicated, may hold values from -3 to 3
- probe_kernel_coefficients: float32 [4, 256], replicated, may hold values from -3 to 3
- cluster_scaling_factor: float32 [1024], replicated, may hold values from 0.1 to 1.9
- emitted_mapping_matrix: bfloat16 [1024, 2048], replicated, may hold values from -0.1875 to 0.1875
- standardize_scaling: float32 [2048], replicated, may hold values from 0.1 to 1.9
- standardize_offset: float32 [2048], replicated, may hold values from -2 to 2
- chosen_specialist_ids: int32 [4, 1024, 2], P('dp', 'sp'), may hold values from 0 to 7, all different within a row; in each aligned block of 128 rows (0 to 127, 128 to 255, ..., all dimensions but the last counted through in order) at most 48 rows name the same one
- specialist_mixing_shares: float32 [4, 1024, 2], P('dp', 'sp'), may hold values from 0.2 to 1
- specialist_gating_matrices: bfloat16 [8, 2048, 5120], P('sp', None, 'dp'), may hold values from -0.125 to 0.125
- raising_matrices: bfloat16 [8, 2048, 5120], P('sp', None, 'dp'), may hold values from -0.125 to 0.125
- lowering_matrices: bfloat16 [8, 5120, 2048], P('sp', 'dp'), may hold values from -0.078125 to 0.078125
Outputs:
- layer_out: bfloat16 [4, 1024, 2048], P('dp', 'sp')
Inputs may be any that keep to these rules, and one draw needn't show every extreme that they name: `chosen_specialist_ids`: each row names two different experts. The rows of one device name no expert more than 48 times, a bound that some block reaches. `channel_fading_speed`: Positive.
All inputs are finite; a program needn't handle non-finite values.
Results may differ from a plain program's by a relative error of at most 0.015.
Values may be sent and summed in bfloat16 or wider, within the bound.
A program may use at most 128 MiB of HBM per device.

v0:
```python
import functools

import jax
import jax.numpy as jnp
from jax import lax
from jax.experimental import pallas as pl
from jax.experimental.pallas import tpu as pltpu
from jax.sharding import PartitionSpec as P

HEADS = 16
HEAD_DIM = 64
GROUPS = 4
STATE = 64
KERNEL = 4
BLK = 128


rms_eps = 1e-06
norm_eps = 1e-05


def causal_conv(series, tap_weights, rim_rows):
    padded = jnp.concatenate([rim_rows, series], axis=0).astype(jnp.float32)
    length = series.shape[0]
    running = jnp.zeros(series.shape, jnp.float32)
    for tap_index in range(tap_weights.shape[0]):
        running = running + tap_weights[tap_index] * lax.slice_in_dim(
            padded, tap_index, tap_index + length, axis=0
        )
    return jax.nn.silu(running).astype(jnp.bfloat16)


def ssd_blocks(x_conv, b_conv, c_conv, increment_delta, fading_exponent, init_state, block_len):
    length, head_count, head_width = x_conv.shape
    state_width = b_conv.shape[2]
    block_count = length // block_len
    x_block = x_conv.reshape(block_count, block_len, head_count, head_width)
    b_block = b_conv.reshape(block_count, block_len, head_count, state_width)
    c_block = c_conv.reshape(block_count, block_len, head_count, state_width)
    cumulative = jnp.cumsum(
        jnp.transpose(fading_exponent.reshape(block_count, block_len, head_count), (0, 2, 1)),
        axis=2,
    )
    step_heads = jnp.transpose(
        increment_delta.reshape(block_count, block_len, head_count), (0, 2, 1)
    )
    causal = jnp.arange(block_len)[:, None] >= jnp.arange(block_len)[None, :]
    within = jnp.exp(
        jnp.where(causal, cumulative[:, :, :, None] - cumulative[:, :, None, :], -jnp.inf)
    )
    scores = jnp.einsum("cthn,cshn->chts", c_block, b_block, preferred_element_type=jnp.float32)
    mixing = (scores * within * step_heads[:, :, None, :]).astype(jnp.bfloat16)
    diag_out = jnp.einsum("chts,cshp->cthp", mixing, x_block, preferred_element_type=jnp.float32)
    tail_decay = jnp.exp(cumulative[:, :, -1:] - cumulative) * step_heads
    scaled = (
        x_block.astype(jnp.float32) * jnp.transpose(tail_decay, (0, 2, 1))[:, :, :, None]
    ).astype(jnp.bfloat16)
    block_state = jnp.einsum("cshp,cshn->chpn", scaled, b_block, preferred_element_type=jnp.float32)
    totals = cumulative[:, :, -1]
    through = jnp.cumsum(totals, axis=0)
    before = through - totals
    earlier = jnp.arange(block_count)[:, None] > jnp.arange(block_count)[None, :]
    carry_weight = jnp.exp(
        jnp.where(earlier[:, :, None], before[:, None, :] - through[None, :, :], -jnp.inf)
    )
    entering = (
        jnp.einsum("cjh,jhpn->chpn", carry_weight, block_state, precision=lax.Precision.HIGHEST)
        + jnp.exp(before)[:, :, None, None] * init_state[None]
    )
    reach_decay = jnp.transpose(jnp.exp(cumulative), (0, 2, 1))
    carried_out = (
        jnp.einsum(
            "cthn,chpn->cthp",
            c_block.astype(jnp.float32),
            entering,
            precision=lax.Precision.HIGHEST,
        )
        * reach_decay[:, :, :, None]
    )
    outcome = (diag_out + carried_out).reshape(length, head_count, head_width)
    final_state = (
        jnp.einsum(
            "jh,jhpn->hpn",
            jnp.exp(through[-1][None, :] - through),
            block_state,
            precision=lax.Precision.HIGHEST,
        )
        + jnp.exp(through[-1])[:, None, None] * init_state
    )
    return (outcome, final_state, through[-1])

MESH = pl.DeviceIdType.MESH


def flip(value, mask):
    result, bit = value, 1
    while bit <= mask:
        if mask & bit:
            result = result + bit * (1 - 2 * ((value // bit) % 2))
        bit *= 2
    return result


def expert_kernel(
    S, R, cap, group, out_ref, wg_hbm, wu_hbm, wd_hbm, ret_ref,
    arr, hid, ra, rx, sx, fin, wg, wu, wd,
    wsem, own_sem, d_s, d_r, g_s, g_r, a_s, a_r, x_s, x_r, b_s, b_r,
):
    s = lax.axis_index("sp")
    d = lax.axis_index("dp")
    nx = R // 2
    steps = S // group
    ahead = 2 // group
    order = list(range(ahead)) + list(range(ahead, steps))
    members = [[p * group + i for i in range(group)] for p in order]
    width = wd.shape[1]
    ff = wg.shape[1]
    f32 = jnp.float32

    def rows(j, dc, dx, count=1):
        return pl.ds((j * R + dc * nx + dx) * cap, count * cap)

    def remote(src, dst, send, recv, where):
        return pltpu.make_async_remote_copy(
            src_ref=src, dst_ref=dst, send_sem=send, recv_sem=recv,
            device_id=where, device_id_type=MESH,
        )

    def disp(j):
        return remote(out_ref.at[pl.ds(j * cap, cap)], arr.at[rows(j, 0, 0)],
                      d_s.at[j], d_r.at[j], {"sp": flip(s, j)})

    def agx(j, dx):
        return remote(arr.at[rows(j, 0, 0)], arr.at[rows(j, 0, dx)],
                      g_s.at[j, dx], g_r.at[j, dx], {"dp": flip(d, 2 * dx)})

    def agc(j, dx):
        return remote(arr.at[rows(j, 0, dx)], arr.at[rows(j, 1, dx)],
                      g_s.at[j, nx + dx], g_r.at[j, nx + dx], {"dp": flip(d, 1)})

    def rsc(j):
        return remote(arr.at[rows(j, 1, 0, nx)], ra.at[pl.ds(j * nx * cap, nx * cap)],
                      a_s.at[j], a_r.at[j], {"dp": flip(d, 1)})

    def rsx(j, dx):
        at = pl.ds((j * (nx - 1) + dx - 1) * cap, cap)
        return remote(sx.at[at], rx.at[at], x_s.at[j, dx], x_r.at[j, dx], {"dp": flip(d, 2 * dx)})

    def back(j):
        return remote(fin.at[pl.ds(j * cap, cap)], ret_ref.at[pl.ds(j * cap, cap)],
                      b_s.at[j], b_r.at[j], {"sp": flip(s, j)})

    own = pltpu.make_async_copy(out_ref.at[pl.ds(0, cap)], arr.at[rows(0, 0, 0)], own_sem)
    loads = [
        pltpu.make_async_copy(src, dst, wsem.at[i])
        for i, (src, dst) in enumerate(((wg_hbm, wg), (wu_hbm, wu), (wd_hbm, wd)))
    ]
    own.start()
    for load in loads:
        load.start()

    barrier = pltpu.get_barrier_semaphore()
    peers = [{"sp": flip(s, j)} for j in range(1, S)]
    peers += [{"dp": flip(d, 1)}] + [{"dp": flip(d, 2 * dx)} for dx in range(1, nx)]
    for peer in peers:
        pl.semaphore_signal(barrier, inc=1, device_id=peer, device_id_type=MESH)
    pl.semaphore_wait(barrier, len(peers))

    for js in members:
        for j in js:
            if j:
                disp(j).start()

    def arrive(p):
        for j in members[p]:
            if j:
                disp(j).wait_recv()
            else:
                own.wait()
            for dx in range(1, nx):
                agx(j, dx).start()
            agc(j, 0).start()

    def relay(p):
        for j in members[p]:
            for dx in range(1, nx):
                agx(j, dx).wait_recv()
                agc(j, dx).start()

    def span(p):
        return pl.ds(order[p] * group * R * cap, group * R * cap)

    def gate_up(p):
        for j in members[p]:
            for dx in range(nx):
                agc(j, dx).wait_recv()
        wide = 256 if ff % 256 == 0 else 128

        def piece(i, carry):
            cols = pl.ds(pl.multiple_of(i * wide, wide), wide)
            x = arr[span(p), :]
            g = jnp.dot(x, wg[:, cols], preferred_element_type=f32)
            u = jnp.dot(x, wu[:, cols], preferred_element_type=f32)
            hid[:, cols] = (jax.nn.silu(g) * u).astype(jnp.bfloat16)
            return carry

        lax.fori_loop(0, ff // wide, piece, 0)

    def down(p):
        for j in members[p]:
            for dx in range(nx):
                if dx:
                    agx(j, dx).wait_send()
                agc(j, dx).wait_send()
        wide = 256 if width % 256 == 0 else 128

        def piece(i, carry):
            cols = pl.ds(pl.multiple_of(i * wide, wide), wide)
            arr[span(p), cols] = jnp.dot(
                hid[...], wd[:, cols], preferred_element_type=f32
            ).astype(jnp.bfloat16)
            return carry

        lax.fori_loop(0, width // wide, piece, 0)
        for j in members[p]:
            rsc(j).start()

    def chip_sum(p):
        for j in members[p]:
            rsc(j).wait_recv()
            for dx in range(1, nx):
                both = (
                    arr[rows(j, 0, dx), :].astype(f32)
                    + ra[pl.ds((j * nx + dx) * cap, cap), :].astype(f32)
                )
                sx[pl.ds((j * (nx - 1) + dx - 1) * cap, cap), :] = both.astype(jnp.bfloat16)
                rsx(j, dx).start()

    def finish(p):
        for j in members[p]:
            total = (
                arr[rows(j, 0, 0), :].astype(f32)
                + ra[pl.ds(j * nx * cap, cap), :].astype(f32)
            )
            for dx in range(1, nx):
                rsx(j, dx).wait_recv()
                total = total + rx[pl.ds((j * (nx - 1) + dx - 1) * cap, cap), :].astype(f32)
            if j:
                fin[pl.ds(j * cap, cap), :] = total.astype(jnp.bfloat16)
                back(j).start()
            else:
                ret_ref[pl.ds(0, cap), :] = total.astype(jnp.bfloat16)

    for p in range(ahead):
        arrive(p)
    loads[0].wait()
    loads[1].wait()
    for p in range(steps):
        relay(p)
        gate_up(p)
        if p + ahead < steps:
            arrive(p + ahead)
        if p == 0:
            loads[2].wait()
        if p > 1:
            finish(p - 2)
        if p:
            chip_sum(p - 1)
        down(p)
    if steps > 1:
        finish(steps - 2)
    chip_sum(steps - 1)
    finish(steps - 1)

    for j in range(S):
        rsc(j).wait_send()
        for dx in range(1, nx):
            rsx(j, dx).wait_send()
        if j:
            disp(j).wait_send()
            back(j).wait_send()
            back(j).wait_recv()


def run_experts(outgoing, gate_w, up_w, down_w, S, R, cap):
    width, ff = gate_w.shape
    nx = R // 2
    group = 1
    bf = jnp.bfloat16
    dma = pltpu.SemaphoreType.DMA
    total = S * R * cap
    return pl.pallas_call(
        functools.partial(expert_kernel, S, R, cap, group),
        out_shape=jax.ShapeDtypeStruct((S * cap, width), bf),
        in_specs=[pl.BlockSpec(memory_space=pltpu.VMEM)]
        + [pl.BlockSpec(memory_space=pl.ANY)] * 3,
        out_specs=pl.BlockSpec(memory_space=pltpu.VMEM),
        scratch_shapes=[
            pltpu.VMEM((total, width), bf),
            pltpu.VMEM((group * R * cap, ff), bf),
            pltpu.VMEM((S * nx * cap, width), bf),
            pltpu.VMEM((S * (nx - 1) * cap, width), bf),
            pltpu.VMEM((S * (nx - 1) * cap, width), bf),
            pltpu.VMEM((S * cap, width), bf),
            pltpu.VMEM((width, ff), bf),
            pltpu.VMEM((width, ff), bf),
            pltpu.VMEM((ff, width), bf),
            dma((3,)), dma(()),
            dma((S,)), dma((S,)),
            dma((S, R)), dma((S, R)),
            dma((S,)), dma((S,)),
            dma((S, nx)), dma((S, nx)),
            dma((S,)), dma((S,)),
        ],
        compiler_params=pltpu.CompilerParams(
            collective_id=0, has_side_effects=True, vmem_limit_bytes=58 * 1024 * 1024
        ),
        cost_estimate=pl.CostEstimate(
            flops=6 * total * width * ff, bytes_accessed=6 * width * ff, transcendentals=total * ff
        ),
    )(outgoing, gate_w, up_w, down_w)


def per_device(
    skip_connection_stream,
    emitted_valve_unscaled,
    channel_source_mapped,
    hidden_source_mapped,
    probe_mapped_values,
    increment_premapped,
    extra_log_fading,
    channel_fading_speed,
    channel_source_kernel,
    hidden_source_kernel,
    probe_kernel_coefficients,
    cluster_scaling_factor,
    emitted_mapping_matrix,
    standardize_scaling,
    standardize_offset,
    chosen_specialist_ids,
    specialist_mixing_shares,
    specialist_gating_matrices,
    raising_matrices,
    lowering_matrices,
):
    sp_size = lax.axis_size("sp")
    sp_index = lax.axis_index("sp")
    tok_rows = skip_connection_stream.shape[1]
    model_width = skip_connection_stream.shape[2]
    inner_width = HEADS * HEAD_DIM
    per_group = HEADS // GROUPS
    head_count = HEADS // sp_size
    first_head = sp_index * head_count
    span = max(1, head_count // per_group)
    copies = max(1, per_group // head_count)
    x_part = channel_source_mapped[0].reshape(tok_rows, sp_size, head_count * HEAD_DIM)
    b_part = hidden_source_mapped[0].reshape(tok_rows, GROUPS // span, span * STATE)
    c_part = probe_mapped_values[0].reshape(tok_rows, GROUPS // span, span * STATE)
    payload = jnp.concatenate(
        [x_part, jnp.repeat(b_part, copies, axis=1), jnp.repeat(c_part, copies, axis=1)], axis=2
    )
    sent_width = payload.shape[2]
    arrived = lax.all_to_all(
        payload.reshape(tok_rows, sp_size * sent_width), "sp", split_axis=1, concat_axis=0, tiled=True
    )
    x_width, s_width = head_count * HEAD_DIM, span * STATE
    state_at = (sp_index // copies) * s_width
    taps = jnp.concatenate(
        [
            lax.dynamic_slice_in_dim(channel_source_kernel, sp_index * x_width, x_width, 1),
            lax.dynamic_slice_in_dim(hidden_source_kernel, state_at, s_width, 1),
            lax.dynamic_slice_in_dim(probe_kernel_coefficients, state_at, s_width, 1),
        ],
        axis=1,
    )
    rim_rows = jnp.zeros((KERNEL - 1, sent_width), jnp.bfloat16)
    flat_conv = causal_conv(arrived, taps, rim_rows)
    seq_rows = flat_conv.shape[0]
    x_conv = flat_conv[:, :x_width].reshape(seq_rows, head_count, HEAD_DIM)
    shared = head_count // span
    b_conv = jnp.repeat(
        flat_conv[:, x_width : x_width + s_width].reshape(seq_rows, span, STATE), shared, axis=1
    )
    c_conv = jnp.repeat(
        flat_conv[:, x_width + s_width :].reshape(seq_rows, span, STATE), shared, axis=1
    )
    increment_delta = jax.nn.softplus(increment_premapped[0])
    speeds_per_channel = lax.dynamic_slice_in_dim(channel_fading_speed, first_head, head_count, 0)
    fading_exponent = extra_log_fading[0] - speeds_per_channel[None, :] * increment_delta
    init_state = jnp.zeros((head_count, HEAD_DIM, STATE), jnp.float32)
    outcome, final_state, total_decay = ssd_blocks(
        x_conv,
        b_conv,
        c_conv,
        increment_delta,
        fading_exponent,
        init_state,
        BLK,
    )
    returned_rows = lax.all_to_all(
        outcome.astype(jnp.bfloat16).reshape(sp_size, tok_rows, x_width),
        "sp",
        split_axis=0,
        concat_axis=0,
        tiled=True,
    )
    blending_outcome = jnp.concatenate([returned_rows[i] for i in range(sp_size)], axis=1)
    gated = blending_outcome.astype(jnp.float32) * jax.nn.silu(
        emitted_valve_unscaled[0].astype(jnp.float32)
    )
    grouped = gated.reshape(tok_rows, GROUPS, inner_width // GROUPS)
    grouped = grouped * lax.rsqrt(jnp.mean(grouped * grouped, axis=-1, keepdims=True) + rms_eps)
    group_normed = (
        grouped.reshape(tok_rows, inner_width) * cluster_scaling_factor[None, :]
    ).astype(jnp.bfloat16)
    pre_norm = skip_connection_stream[0].astype(jnp.float32) + jnp.dot(
        group_normed, emitted_mapping_matrix, preferred_element_type=jnp.float32
    )
    centre = jnp.mean(pre_norm, axis=-1, keepdims=True)
    variance = jnp.mean(jnp.square(pre_norm - centre), axis=-1, keepdims=True)
    normed = (
        (pre_norm - centre) * lax.rsqrt(variance + norm_eps) * standardize_scaling[None, :]
        + standardize_offset[None, :]
    ).astype(jnp.bfloat16)
    slot_cap = -(-(3 * tok_rows // sp_size) // 16) * 16
    dp_size = lax.axis_size("dp")
    slots = sp_size * slot_cap
    flat_ids = chosen_specialist_ids[0].reshape(-1)
    matched = (flat_ids[:, None] == jnp.arange(sp_size, dtype=jnp.int32)[None, :]).astype(jnp.int32)
    ranked = jnp.cumsum(matched, axis=0) - 1
    relative = jnp.bitwise_xor(flat_ids, sp_index)
    target = (relative * slot_cap + jnp.sum(matched * ranked, axis=1)).reshape(tok_rows, 2)
    placing = jnp.arange(slots, dtype=jnp.int32)[:, None]
    placing = ((placing == target[None, :, 0]) | (placing == target[None, :, 1])).astype(jnp.bfloat16)
    outgoing = jnp.dot(placing, normed, preferred_element_type=jnp.float32).astype(jnp.bfloat16)
    answered = run_experts(
        outgoing,
        specialist_gating_matrices[0],
        raising_matrices[0],
        lowering_matrices[0],
        sp_size,
        dp_size,
        slot_cap,
    )
    slot_index = jnp.arange(slots, dtype=jnp.int32)[None, :]
    routed_sum = jnp.zeros((tok_rows, model_width), jnp.float32)
    for choice in range(2):
        picking = (slot_index == target[:, choice : choice + 1]).astype(jnp.bfloat16)
        routed_sum = routed_sum + specialist_mixing_shares[0][:, choice : choice + 1] * jnp.dot(
            picking, answered, preferred_element_type=jnp.float32
        )
    layer_out = (normed.astype(jnp.float32) + routed_sum).astype(jnp.bfloat16)
    return layer_out[None]


def solution(mesh):
    placed = (
        P("dp", "sp", None),
        P("dp", "sp", None),
        P("dp", "sp", None),
        P("dp", "sp", None),
        P("dp", "sp", None),
        P("dp", None, "sp"),
        P("dp", None, "sp"),
        P(),
        P(),
        P(),
        P(),
        P(),
        P(),
        P(),
        P(),
        P("dp", "sp", None),
        P("dp", "sp", None),
        P("sp", None, "dp"),
        P("sp", None, "dp"),
        P("sp", "dp", None),
    )
    return jax.shard_map(
        per_device, mesh=mesh, in_specs=placed, out_specs=P("dp", "sp", None), check_vma=False
    )
```

profile of v0, /device:TPU:8, one launch (start us, length us, event | category | flops | bytes accessed | tf_op | source)
XLA Modules:
  0.0 155.5 jit_solution(1597718533847358438)
XLA Ops:
  0.0 1.2 copy.90
  1.2 1.0 copy.91
  2.2 1.0 copy.92
  3.2 0.8 pad_maximum_fusion
  4.0 6.3 %all-to-all-start = ((bf16[128,8,256]{0,2,1:T(8,128)(2,1)}), bf16[128,8,256]{0,2,1:T(8,128)(2,1)S(1)}, u32[]{:S(2)}, u32[]{:S(2)}) async-start(bf16[128,8,256]{0,2,1:T(8,128)(2,1)} %pad_maximum_fusion), calls=%async_computation | async-start | bytes 1048576 | tf_op jit(solution)/shard_map/all_to_all | solution.py:363
  10.5 0.6 reduce_window_sum.35
  11.7 0.6 reduce-window.6
  13.3 10.2 %all-to-all-done = bf16[128,8,256]{0,2,1:T(8,128)(2,1)S(1)} async-done(((bf16[128,8,256]{0,2,1:T(8,128)(2,1)}), bf16[128,8,256]{0,2,1:T(8,128)(2,1)S(1)}, u32[]{:S(2)}, u32[]{:S(2)}) %all-to-all-start) | async-done | bytes 524320 | tf_op jit(solution)/shard_map/all_to_all | solution.py:363
  23.9 0.6 multiply_convert_fusion
  25.2 0.3 fusion.34
  25.5 0.9 fusion.6
  26.4 0.4 fusion.8
  26.8 0.8 fusion.9
  27.7 0.9 copy.106
  28.5 4.9 %all-to-all-start.1 = ((bf16[8,128,128]{2,1,0:T(8,128)(2,1)}), bf16[8,128,128]{2,1,0:T(8,128)(2,1)S(1)}, u32[]{:S(2)}, u32[]{:S(2)}) async-start(bf16[8,128,128]{2,1,0:T(8,128)(2,1)} %copy.106), calls=%async_computation.1 | async-start | bytes 524288 | tf_op jit(solution)/shard_map/all_to_all | solution.py:400
  33.7 7.9 %all-to-all-done.1 = bf16[8,128,128]{2,1,0:T(8,128)(2,1)S(1)} async-done(((bf16[8,128,128]{2,1,0:T(8,128)(2,1)}), bf16[8,128,128]{2,1,0:T(8,128)(2,1)S(1)}, u32[]{:S(2)}, u32[]{:S(2)}) %all-to-all-start.1) | async-done | bytes 262176 | tf_op jit(solution)/shard_map/all_to_all | solution.py:400
  41.9 0.4 fusion.32
  42.7 0.2 copy-done.11
  43.0 3.1 %fusion.82 = (f32[128]{0:T(128)S(1)}, f32[128,2048]{1,0:T(8,128)S(1)}) fusion(bf16[1024,2048]{1,0:T(8,128)(2,1)} %param.32, f32[128,1024]{1,0:T(8,128)S(1)} %bitcast.173, f32[1024]{0:T(1024)S(1)} %copy-done.12, bf16[1,128,1024]{2,1,0:T(8,128)(2,1)S(1)} %copy-done.2, bf16[128,1024]{1,0:T(8,128)(2,1)S(1)} %fusion.53, bf16[1,128,2048]{2,1,0:T(8,128)(2,1)S(1)} %copy-done.11), kind=kOutput, calls=%fused_computation.137 | convolution fusion | flops 538967936 | bytes 6820352 | tf_op jit(solution)/shard_map/dot_general | solution.py:416
  46.1 0.3 multiply_reduce_fusion
  46.4 1.8 %convolution_convert_fusion.out_ref = bf16[384,2048]{1,0:T(8,128)(2,1)} fusion(s32[128]{0:T(128)S(1)} %get-tuple-element.18, s32[128]{0:T(128)S(1)} %get-tuple-element.17, f32[128,2048]{1,0:T(8,128)S(1)} %get-tuple-element.20, f32[2048]{0:T(1024)S(1)} %copy-done.3, f32[2048]{0:T(1024)S(1)} %copy-done.4, f32[128]{0:T(128)S(1)} %add_rsqrt_fusion.1, ...), kind=kOutput, calls=%fused_computation | convolution fusion | flops 203571200 | bytes 2639872 | tf_op jit(solution)/shard_map/dot_general | solution.py:435
  48.2 103.8 %shard_map.190 = bf16[384,2048]{1,0:T(8,128)(2,1)} custom-call(bf16[384,2048]{1,0:T(8,128)(2,1)} %convolution_convert_fusion.out_ref, bf16[2048,1280]{1,0:T(8,128)(2,1)} %bitcast.187, bf16[2048,1280]{1,0:T(8,128)(2,1)} %bitcast.188, bf16[1280,2048]{1,0:T(8,128)(2,1)} %bitcast.189), custom_call_target="tpu_custom_call" | custom-call | flops 24159191040 | bytes 15728640 | tf_op jit(solution)/shard_map/pallas_call | solution.py:292
  152.0 2.0 %convolution_multiply_fusion.1 = f32[128,2048]{1,0:T(8,128)S(1)} fusion(bf16[384,2048]{1,0:T(8,128)(2,1)} %shard_map.190, f32[128]{0:T(128)S(1)} %get-tuple-element.16, s32[128]{0:T(128)S(1)} %get-tuple-element.17), kind=kOutput, calls=%fused_computation.4 | convolution fusion | flops 201637888 | bytes 2622464 | tf_op jit(solution)/shard_map/dot_general | solution.py:449
  154.1 1.4 fusion.3
  (82 shorter events, 3.7 us)
Async XLA Ops:
  0.0 13.1 %copy-start = (f32[4,1024]{1,0:T(4,128)S(1)}, f32[4,1024]{1,0:T(4,128)}, u32[]{:S(2)}) copy-start(f32[4,1024]{1,0:T(4,128)} %param.28) | copy-start | bytes 49156
  0.0 10.3 %copy-start.13 = (f32[16]{0:T(128)S(1)}, f32[16]{0:T(128)}, u32[]{:S(2)}) copy-start(f32[16]{0:T(128)} %param.27) | copy-start | bytes 196
  0.0 10.4 %copy-start.5 = (f32[1,1024,2]{1,2,0:T(2,128)S(1)}, f32[1,1024,2]{1,2,0:T(2,128)}, u32[]{:S(2)}) copy-start(f32[1,1024,2]{1,2,0:T(2,128)} %param.25) | copy-start | bytes 24580
  0.0 10.4 %copy-start.6 = (f32[1,1024,2]{1,2,0:T(2,128)S(1)}, f32[1,1024,2]{1,2,0:T(2,128)}, u32[]{:S(2)}) copy-start(f32[1,1024,2]{1,2,0:T(2,128)} %param.26) | copy-start | bytes 24580
  0.0 11.2 %copy-start.7 = (s32[1,128,2]{1,2,0:T(2,128)S(1)}, s32[1,128,2]{1,2,0:T(2,128)}, u32[]{:S(2)}) copy-start(s32[1,128,2]{1,2,0:T(2,128)} %param.35) | copy-start | bytes 3076
  3.1 10.0 %copy-start.8 = (f32[4,256]{1,0:T(4,128)S(1)}, f32[4,256]{1,0:T(4,128)}, u32[]{:S(2)}) copy-start(f32[4,256]{1,0:T(4,128)} %param.30) | copy-start | bytes 12292
  3.1 10.0 %copy-start.9 = (f32[4,256]{1,0:T(4,128)S(1)}, f32[4,256]{1,0:T(4,128)}, u32[]{:S(2)}) copy-start(f32[4,256]{1,0:T(4,128)} %param.29) | copy-start | bytes 12292
  4.0 19.5 %all-to-all-start = ((bf16[128,8,256]{0,2,1:T(8,128)(2,1)}), bf16[128,8,256]{0,2,1:T(8,128)(2,1)S(1)}, u32[]{:S(2)}, u32[]{:S(2)}) async-start(bf16[128,8,256]{0,2,1:T(8,128)(2,1)} %pad_maximum_fusion), calls=%async_computation | async-start | bytes 1048576 | tf_op jit(solution)/shard_map/all_to_all | solution.py:363
  26.8 6.6 %copy-start.2 = (bf16[1,128,1024]{2,1,0:T(8,128)(2,1)S(1)}, bf16[1,128,1024]{2,1,0:T(8,128)(2,1)}, u32[]{:S(2)}) copy-start(bf16[1,128,1024]{2,1,0:T(8,128)(2,1)} %param.21) | copy-start | bytes 786436
  26.8 6.9 %copy-start.10 = (f32[1,128,2]{1,2,0:T(2,128)S(1)}, f32[1,128,2]{1,2,0:T(2,128)}, u32[]{:S(2)}) copy-start(f32[1,128,2]{1,2,0:T(2,128)} %param.36) | copy-start | bytes 3076
  28.5 13.0 %all-to-all-start.1 = ((bf16[8,128,128]{2,1,0:T(8,128)(2,1)}), bf16[8,128,128]{2,1,0:T(8,128)(2,1)S(1)}, u32[]{:S(2)}, u32[]{:S(2)}) async-start(bf16[8,128,128]{2,1,0:T(8,128)(2,1)} %copy.106), calls=%async_computation.1 | async-start | bytes 524288 | tf_op jit(solution)/shard_map/all_to_all | solution.py:400
  41.9 1.0 copy-start.11
  41.9 1.0 copy-start.12
  43.0 3.4 %copy-start.3 = (f32[2048]{0:T(1024)S(1)}, f32[2048]{0:T(1024)}, u32[]{:S(2)}) copy-start(f32[2048]{0:T(1024)} %param.34) | copy-start | bytes 24580
  43.0 3.4 %copy-start.4 = (f32[2048]{0:T(1024)S(1)}, f32[2048]{0:T(1024)}, u32[]{:S(2)}) copy-start(f32[2048]{0:T(1024)} %param.33) | copy-start | bytes 24580
  152.0 2.0 %copy-start.1 = (bf16[384,2048]{1,0:T(8,128)(2,1)S(1)}, bf16[384,2048]{1,0:T(8,128)(2,1)}, u32[]{:S(2)}) copy-start(bf16[384,2048]{1,0:T(8,128)(2,1)} %shard_map.190) | copy-start | bytes 4718596
where the time goes:
time: 157 us; the launch traced here: 155 us
  Pallas kernels  104 us (66%)
  waiting for transfers between devices  18.1 us (12%)
  starting transfers between devices  11.2 us (7%)
  matrix products  10.7 us (7%)
  local copies, waits for them, and re-layouts  7.14 us (5%)
  other arithmetic  4.09 us (3%)
    pallas_call x1, Pallas kernels, run_experts(): pl.pallas_call(functools.partial(expert_kernel, S, R, cap, group), out_sh...  104 us
    all_to_all x1, waiting for transfers between devices, per_device(): lax.all_to_all(payload.reshape(tok_rows, sp_size * sent_width), 'sp', spl...  10.2 us
    all_to_all x1, waiting for transfers between devices, per_device(): lax.all_to_all(outcome.astype(jnp.bfloat16).reshape(sp_size, tok_rows, x_...  7.86 us
    all_to_all x1, starting transfers between devices, per_device(): lax.all_to_all(payload.reshape(tok_rows, sp_size * sent_width), 'sp', spl...  6.28 us
    all_to_all x1, starting transfers between devices, per_device(): lax.all_to_all(outcome.astype(jnp.bfloat16).reshape(sp_size, tok_rows, x_...  4.9 us
    unnamed x41, local copies, waits for them, and re-layouts  3.73 us
    dot_general x2, matrix products, per_device(): jnp.dot(picking, answered, preferred_element_type=jnp.float32)  3.41 us
  transfers between devices with their start and end apart: 2, of which 2 were waited for; matrix products, arithmetic and copies ran while one was open for 2% of the time, Pallas kernels for 0%

commit v1 on v0

v1 whole, which is shorter than its diff:
```python
import functools

import jax
import jax.numpy as jnp
from jax import lax
from jax.experimental import pallas as pl
from jax.experimental.pallas import tpu as pltpu
from jax.sharding import PartitionSpec as P

HEADS = 16
HEAD_DIM = 64
GROUPS = 4
STATE = 64
KERNEL = 4
BLK = 128

RMS_EPS = 1e-06
NORM_EPS = 1e-05
HALO = 16
MESH = pl.DeviceIdType.MESH
F32 = jnp.float32
BF16 = jnp.bfloat16
I32 = jnp.int32


def flip(value, mask):
    result, bit = value, 1
    while bit <= mask:
        if mask & bit:
            result = result + bit * (1 - 2 * ((value // bit) % 2))
        bit *= 2
    return result


def iota(shape, dim):
    return lax.broadcasted_iota(I32, shape, dim)


def lane_scan(value, width):
    lanes = iota(value.shape, 1)
    step = 1
    while step < width:
        value = value + jnp.where(lanes >= step, pltpu.roll(value, step, 1), 0.0)
        step *= 2
    return value


def layer_kernel(
    S, R, Y, cap,
    xs_hbm, bs_hbm, cs_hbm, valve_hbm, skip_hbm, wo_hbm, wg_hbm, wu_hbm, wd_hbm,
    inc_ref, fade_ref, speed_ref, xk_ref, bk_ref, ck_ref, gain_ref, lns_ref, lno_ref,
    ids_ref, share_ref,
    out_ref,
    joined, conv, valve, skip, wo, msg, rbuf, step_rows, decay_rows, total_rows, rows, cols,
    cmask, diag, scaled, state, sendz, recvz, sendy, recvy, normed_g, pre, normed,
    outb, arr, hid, ra, rx, sx, ret, wg, wu, wd,
    in_sem, w_sem, m_s, m_r, h_s, h_r, z_s, z_r, y_s, y_r,
    d_s, d_r, g_s, g_r, a_s, a_r, x_s, x_r, b_s, b_r,
):
    s = lax.axis_index("sp")
    d = lax.axis_index("dp")
    T, inner = xs_hbm.shape
    span = bs_hbm.shape[1]
    width = skip_hbm.shape[1]
    ff = wg_hbm.shape[1]
    hc = inc_ref.shape[0]
    H = HEADS
    G = GROUPS
    gw = inner // G
    pair = 2 * HEAD_DIM
    zi = s // Y
    yi = s % Y
    Z = S // Y
    nx = R // 2

    def remote(src, dst, send, recv, where):
        return pltpu.make_async_remote_copy(
            src_ref=src, dst_ref=dst, send_sem=send, recv_sem=recv,
            device_id=where, device_id_type=MESH,
        )

    def local(src, dst, sem):
        return pltpu.make_async_copy(src, dst, sem)

    body = pl.ds(HALO, T)
    loads = [
        local(xs_hbm, joined.at[body, pl.ds(0, inner)], in_sem.at[0]),
        local(bs_hbm, joined.at[body, pl.ds(inner, span)], in_sem.at[1]),
        local(cs_hbm, joined.at[body, pl.ds(inner + span, span)], in_sem.at[2]),
        local(valve_hbm, valve, in_sem.at[3]),
        local(skip_hbm, skip, in_sem.at[4]),
        local(wo_hbm, wo, in_sem.at[5]),
    ]
    weights = [
        local(src, dst, w_sem.at[i])
        for i, (src, dst) in enumerate(((wg_hbm, wg), (wu_hbm, wu), (wd_hbm, wd)))
    ]
    for load in loads:
        load.start()

    barrier = pltpu.get_barrier_semaphore()
    peers = [{"sp": flip(s, j)} for j in range(1, S)]
    peers += [{"dp": flip(d, 1)}] + [{"dp": flip(d, 2 * dx)} for dx in range(1, nx)]
    for peer in peers:
        pl.semaphore_signal(barrier, inc=1, device_id=peer, device_id_type=MESH)

    step_in = jax.nn.softplus(inc_ref[...])
    own_rows = iota((hc, 1), 0)
    speeds = jnp.zeros((hc, 1), F32)
    for i in range(hc):
        speeds = jnp.where(own_rows == i, speed_ref[s * hc + i], speeds)
    decay_in = fade_ref[...] - speeds * step_in
    tot_lanes = iota((hc, T), 1)
    totals_in = jnp.zeros((hc, T), F32)
    for j in range(S):
        block = decay_in[:, j * T : (j + 1) * T]
        totals_in = jnp.where(tot_lanes == j, jnp.sum(block, axis=1, keepdims=True), totals_in)
    for j in range(S):
        msg[j, pl.ds(0, hc), :] = step_in[:, j * T : (j + 1) * T]
        msg[j, pl.ds(hc, hc), :] = decay_in[:, j * T : (j + 1) * T]
        msg[j, pl.ds(2 * hc, hc), :] = totals_in
        msg[j, pl.ds(3 * hc, 8 - 3 * hc), :] = jnp.zeros((8 - 3 * hc, T), F32)

    pl.semaphore_wait(barrier, len(peers))

    def share_steps(j):
        return remote(msg.at[flip(s, j)], rbuf.at[s], m_s.at[j], m_r.at[j], {"sp": flip(s, j)})

    def halo_to():
        return remote(
            joined.at[pl.ds(T, HALO)], joined.at[pl.ds(0, HALO)], h_s, h_r, {"sp": s + 1}
        )

    for j in range(S - 1, 0, -1):
        share_steps(j).start()
    rbuf[s] = msg[s]

    for load in loads[:3]:
        load.wait()

    @pl.when(s < S - 1)
    def _():
        halo_to().start()

    for load in weights:
        load.start()

    @pl.when(s == 0)
    def _():
        joined[pl.ds(0, HALO), :] = jnp.zeros((HALO, joined.shape[1]), BF16)

    @pl.when(zi == 0)
    def _():
        recvz[...] = jnp.zeros(recvz.shape, BF16)

    experts = iota((S, T), 0)
    hot = [(ids_ref[k : k + 1, :] == experts) for k in range(2)]
    named = (hot[0].astype(F32) + hot[1].astype(F32)).astype(BF16)
    before_t = (iota((T, T), 0) < iota((T, T), 1)).astype(F32).astype(BF16)
    ranks = jnp.dot(named, before_t, preferred_element_type=F32)
    targets = []
    for k in range(2):
        rank = jnp.sum(jnp.where(hot[k], ranks, 0.0), axis=0, keepdims=True)
        relative = jnp.bitwise_xor(ids_ref[k : k + 1, :], s)
        targets.append(relative * cap + rank.astype(I32))
        rows[3 * H + k : 3 * H + k + 1, :] = targets[k].astype(F32)
    rows[3 * H + 2 :, :] = jnp.zeros((rows.shape[0] - 3 * H - 2, T), F32)

    @pl.when(s > 0)
    def _():
        halo_to().wait_recv()

    chunk = 256
    first = HALO - KERNEL + 1
    for taps, at in ((xk_ref, 0), (bk_ref, inner), (ck_ref, inner + span)):
        for c in range(0, taps.shape[1], chunk):
            series = joined[:, at + c : at + c + chunk].astype(F32)
            total = jnp.zeros((T, chunk), F32)
            for k in range(KERNEL):
                total = total + taps[k : k + 1, c : c + chunk] * series[first + k : first + k + T, :]
            conv[:, at + c : at + c + chunk] = jax.nn.silu(total).astype(BF16)

    for j in range(1, S):
        share_steps(j).wait_recv()
    for p in range(S):
        at = pl.ds(p * hc, hc)
        step_rows[at, :] = rbuf[p, pl.ds(0, hc), :]
        decay_rows[at, :] = rbuf[p, pl.ds(hc, hc), :]
        total_rows[at, :] = rbuf[p, pl.ds(2 * hc, hc), :]
    steps = step_rows[...]
    cumulative = lane_scan(decay_rows[...], T)
    final = jnp.sum(jnp.where(iota((H, T), 1) == T - 1, cumulative, 0.0), axis=1, keepdims=True)
    rows[0:H, :] = cumulative
    rows[H : 2 * H, :] = jnp.exp(final - cumulative) * steps
    rows[2 * H : 3 * H, :] = jnp.exp(cumulative)
    cols[...] = rows[...].T

    lane = iota((T, pair), 1)
    low = lane < HEAD_DIM

    def by_head(base, q):
        return jnp.where(
            low, cols[:, base + 2 * q : base + 2 * q + 1], cols[:, base + 2 * q + 1 : base + 2 * q + 2]
        )

    for q in range(H // 2):
        at = pl.ds(q * pair, pair)
        scaled[:, at] = (conv[:, at].astype(F32) * by_head(H, q)).astype(BF16)
    for p in range(G // 2):
        b_pair = conv[:, inner + p * pair : inner + (p + 1) * pair]
        both = lax.dot_general(
            b_pair, scaled[:, 2 * gw * p : 2 * gw * (p + 1)], (((0,), (0,)), ((), ())),
            preferred_element_type=F32,
        )
        for i in range(2):
            state[2 * p + i] = both[i * STATE : (i + 1) * STATE, i * gw : (i + 1) * gw]

    lanes_h = iota((H, T), 1)
    through = lane_scan(total_rows[...], S)
    ahead_of = through - total_rows[...]

    def pick(values, index):
        return jnp.sum(jnp.where(lanes_h == index, values, 0.0), axis=1, keepdims=True)

    head_of = iota((H, inner), 1) // HEAD_DIM == iota((H, inner), 0)

    def spread(column):
        return jnp.sum(jnp.where(head_of, column, 0.0), axis=0, keepdims=True)

    at_plane = pick(ahead_of, zi * Y)
    at_next = pick(ahead_of, zi * Y + Y)
    at_here = pick(ahead_of, s)
    past_here = pick(through, s)
    zf = spread(jnp.exp(at_next - at_plane))
    zs = spread(jnp.exp(at_next - past_here))
    own_f = spread(jnp.exp(at_here - at_plane))
    yf, ys = [None], [None]
    for dy in range(1, Y):
        at_peer = pick(ahead_of, flip(s, dy))
        later = flip(s, dy) > s
        yf.append(spread(jnp.exp(at_peer - at_plane)))
        ys.append(spread(jnp.where(later, jnp.exp(jnp.minimum(at_peer - past_here, 0.0)), 0.0)))

    def column(values, g):
        return values[:, g * gw : (g + 1) * gw]

    def along_z(g):
        return remote(sendz.at[g], recvz.at[g], z_s.at[g], z_r.at[g], {"sp": s + Y})

    def along_y(dy, g):
        return remote(
            sendy.at[dy - 1, g], recvy.at[dy - 1, g], y_s.at[dy - 1, g], y_r.at[dy - 1, g],
            {"sp": flip(s, dy)},
        )

    @pl.when(zi == 0)
    def _():
        for g in range(G):
            sendz[g] = (column(zs, g) * state[g]).astype(BF16)
            along_z(g).start()

    causal = iota((T, T), 0) >= iota((T, T), 1)
    for g in range(G):
        p, i = g // 2, g % 2
        at_b = inner + p * pair
        at_c = inner + span + p * pair
        half = low if i == 0 else jnp.logical_not(low)
        c_half = jnp.where(half, conv[:, at_c : at_c + pair].astype(F32), 0.0).astype(BF16)
        cmask[g] = c_half
        scores = lax.dot_general(
            c_half, conv[:, at_b : at_b + pair], (((1,), (1,)), ((), ())),
            preferred_element_type=F32,
        )
        per = H // G // 2
        for q in range(g * per, (g + 1) * per):
            at = pl.ds(q * pair, pair)
            mixes = []
            for h in (2 * q, 2 * q + 1):
                gap = jnp.where(causal, cols[:, h : h + 1] - rows[h : h + 1, :], -jnp.inf)
                mixes.append((scores * jnp.exp(gap) * step_rows[h : h + 1, :]).astype(BF16))
            x_pair = conv[:, at].astype(F32)
            stacked = jnp.concatenate(
                [jnp.where(low, x_pair, 0.0).astype(BF16), jnp.where(low, 0.0, x_pair).astype(BF16)],
                axis=0,
            )
            diag[:, at] = jnp.dot(
                jnp.concatenate(mixes, axis=1), stacked, preferred_element_type=F32
            )

    for g in range(G):
        @pl.when(zi > 0)
        def _():
            along_z(g).wait_recv()

        @pl.when(jnp.logical_and(zi > 0, zi < Z - 1))
        def _():
            sendz[g] = (column(zf, g) * recvz[g].astype(F32) + column(zs, g) * state[g]).astype(BF16)
            along_z(g).start()

        for dy in range(1, Y):
            sendy[dy - 1, g] = (
                column(yf[dy], g) * recvz[g].astype(F32) + column(ys[dy], g) * state[g]
            ).astype(BF16)
            along_y(dy, g).start()

    for load in loads[3:]:
        load.wait()
    for g in range(G):
        at = pl.ds(g * gw, gw)
        entering = column(own_f, g) * recvz[g].astype(F32)
        for dy in range(1, Y):
            along_y(dy, g).wait_recv()
            entering = entering + recvy[dy - 1, g].astype(F32)
        high = entering.astype(BF16)
        rest = (entering - high.astype(F32)).astype(BF16)
        c_half = cmask[g]
        carried = jnp.dot(
            c_half, jnp.concatenate([high, high], axis=0), preferred_element_type=F32
        ) + jnp.dot(c_half, jnp.concatenate([rest, rest], axis=0), preferred_element_type=F32)
        per = H // G // 2
        reach = jnp.concatenate([by_head(2 * H, q) for q in range(g * per, (g + 1) * per)], axis=1)
        mixed = (diag[:, at] + carried * reach).astype(BF16)
        gated = mixed.astype(F32) * jax.nn.silu(valve[:, at].astype(F32))
        power = jnp.mean(gated * gated, axis=-1, keepdims=True)
        normed_g[:, at] = (gated * lax.rsqrt(power + RMS_EPS) * gain_ref[:, at]).astype(BF16)
        base = skip[...].astype(F32) if g == 0 else pre[...]
        pre[...] = base + jnp.dot(normed_g[:, at], wo[at, :], preferred_element_type=F32)

    tile = 16

    def normalise(i, carry):
        at = pl.ds(pl.multiple_of(i * tile, tile), tile)
        value = pre[at, :]
        centre = jnp.mean(value, axis=-1, keepdims=True)
        gap = value - centre
        variance = jnp.mean(gap * gap, axis=-1, keepdims=True)
        normed[at, :] = (
            gap * lax.rsqrt(variance + NORM_EPS) * lns_ref[...] + lno_ref[...]
        ).astype(BF16)
        return carry

    lax.fori_loop(0, T // tile, normalise, 0)

    order = list(range(S))
    ahead = 2

    def slot_rows(j, dc, dx, count=1):
        return pl.ds((j * R + dc * nx + dx) * cap, count * cap)

    def disp(j):
        return remote(outb.at[pl.ds(j * cap, cap)], arr.at[slot_rows(j, 0, 0)],
                      d_s.at[j], d_r.at[j], {"sp": flip(s, j)})

    def agx(j, dx):
        return remote(arr.at[slot_rows(j, 0, 0)], arr.at[slot_rows(j, 0, dx)],
                      g_s.at[j, dx], g_r.at[j, dx], {"dp": flip(d, 2 * dx)})

    def agc(j, dx):
        return remote(arr.at[slot_rows(j, 0, dx)], arr.at[slot_rows(j, 1, dx)],
                      g_s.at[j, nx + dx], g_r.at[j, nx + dx], {"dp": flip(d, 1)})

    def rsc(j):
        return remote(arr.at[slot_rows(j, 1, 0, nx)], ra.at[pl.ds(j * nx * cap, nx * cap)],
                      a_s.at[j], a_r.at[j], {"dp": flip(d, 1)})

    def rsx(j, dx):
        at = pl.ds((j * (nx - 1) + dx - 1) * cap, cap)
        return remote(sx.at[at], rx.at[at], x_s.at[j, dx], x_r.at[j, dx], {"dp": flip(d, 2 * dx)})

    def back(j):
        return remote(outb.at[pl.ds(j * cap, cap)], ret.at[pl.ds(j * cap, cap)],
                      b_s.at[j], b_r.at[j], {"sp": flip(s, j)})

    def place(j):
        slot = iota((cap, T), 0) + j * cap
        hit = jnp.logical_or(slot == targets[0], slot == targets[1])
        moved = jnp.dot(
            hit.astype(F32).astype(BF16), normed[...], preferred_element_type=F32
        ).astype(BF16)
        if j:
            outb[pl.ds(j * cap, cap), :] = moved
            disp(j).start()
        else:
            arr[slot_rows(0, 0, 0), :] = moved

    for j in order:
        place(j)

    def arrive(j):
        if j:
            disp(j).wait_recv()
        for dx in range(1, nx):
            agx(j, dx).start()
        agc(j, 0).start()

    def relay(j):
        for dx in range(1, nx):
            agx(j, dx).wait_recv()
            agc(j, dx).start()

    def gate_up(j):
        for dx in range(nx):
            agc(j, dx).wait_recv()
        wide = 256 if ff % 256 == 0 else 128

        def piece(i, carry):
            at = pl.ds(pl.multiple_of(i * wide, wide), wide)
            x = arr[slot_rows(j, 0, 0, R), :]
            g = jnp.dot(x, wg[:, at], preferred_element_type=F32)
            u = jnp.dot(x, wu[:, at], preferred_element_type=F32)
            hid[:, at] = (jax.nn.silu(g) * u).astype(BF16)
            return carry

        lax.fori_loop(0, ff // wide, piece, 0)

    def down(j):
        for dx in range(nx):
            if dx:
                agx(j, dx).wait_send()
            agc(j, dx).wait_send()
        wide = 256 if width % 256 == 0 else 128

        def piece(i, carry):
            at = pl.ds(pl.multiple_of(i * wide, wide), wide)
            arr[slot_rows(j, 0, 0, R), at] = jnp.dot(
                hid[...], wd[:, at], preferred_element_type=F32
            ).astype(BF16)
            return carry

        lax.fori_loop(0, width // wide, piece, 0)
        rsc(j).start()

    def chip_sum(j):
        rsc(j).wait_recv()
        for dx in range(1, nx):
            both = (
                arr[slot_rows(j, 0, dx), :].astype(F32)
                + ra[pl.ds((j * nx + dx) * cap, cap), :].astype(F32)
            )
            sx[pl.ds((j * (nx - 1) + dx - 1) * cap, cap), :] = both.astype(BF16)
            rsx(j, dx).start()

    def finish(j):
        total = (
            arr[slot_rows(j, 0, 0), :].astype(F32)
            + ra[pl.ds(j * nx * cap, cap), :].astype(F32)
        )
        for dx in range(1, nx):
            rsx(j, dx).wait_recv()
            total = total + rx[pl.ds((j * (nx - 1) + dx - 1) * cap, cap), :].astype(F32)
        if j:
            disp(j).wait_send()
            outb[pl.ds(j * cap, cap), :] = total.astype(BF16)
            back(j).start()
        else:
            ret[pl.ds(0, cap), :] = total.astype(BF16)

    for j in order[:ahead]:
        arrive(j)
    weights[0].wait()
    weights[1].wait()
    for p, j in enumerate(order):
        relay(j)
        gate_up(j)
        if p + ahead < S:
            arrive(order[p + ahead])
        if p == 0:
            weights[2].wait()
        if p > 1:
            finish(order[p - 2])
        if p:
            chip_sum(order[p - 1])
        down(j)
    if S > 1:
        finish(order[S - 2])
    chip_sum(order[S - 1])
    finish(order[S - 1])

    target_cols = [cols[:, 3 * H + k : 3 * H + k + 1].astype(I32) for k in range(2)]
    shares = [share_ref[:, k : k + 1] for k in range(2)]
    pre[...] = normed[...].astype(F32)
    for j in order:
        if j:
            back(j).wait_recv()
        slot = iota((T, cap), 1) + j * cap
        hit = jnp.logical_or(slot == target_cols[0], slot == target_cols[1])
        share = jnp.zeros((T, 1), F32)
        for k in range(2):
            inside = jnp.logical_and(target_cols[k] >= j * cap, target_cols[k] < (j + 1) * cap)
            share = share + jnp.where(inside, shares[k], 0.0)
        moved = jnp.dot(
            hit.astype(F32).astype(BF16), ret[pl.ds(j * cap, cap), :], preferred_element_type=F32
        )
        pre[...] = pre[...] + share * moved
    out_ref[...] = pre[...].astype(BF16)

    for j in range(1, S):
        share_steps(j).wait_send()

    @pl.when(s < S - 1)
    def _():
        halo_to().wait_send()

    @pl.when(zi < Z - 1)
    def _():
        for g in range(G):
            along_z(g).wait_send()

    for g in range(G):
        for dy in range(1, Y):
            along_y(dy, g).wait_send()
    for j in range(S):
        rsc(j).wait_send()
        for dx in range(1, nx):
            rsx(j, dx).wait_send()
        if j:
            back(j).wait_send()


def run_layer(S, R, cap, big, small):
    xs, bs, cs, valve, skip, wo, wg, wu, wd = big
    T, inner = xs.shape
    span = bs.shape[1]
    width = skip.shape[1]
    ff = wg.shape[1]
    nx = R // 2
    Y = 1
    while Y * Y * 4 <= S:
        Y *= 2
    gw = inner // GROUPS
    dma = pltpu.SemaphoreType.DMA
    vmem = pltpu.VMEM
    total = S * R * cap
    whole = inner + 2 * span
    return pl.pallas_call(
        functools.partial(layer_kernel, S, R, Y, cap),
        out_shape=jax.ShapeDtypeStruct((T, width), BF16),
        in_specs=[pl.BlockSpec(memory_space=pl.ANY)] * 9
        + [pl.BlockSpec(memory_space=pltpu.VMEM)] * 2
        + [pl.BlockSpec(memory_space=pltpu.SMEM)]
        + [pl.BlockSpec(memory_space=pltpu.VMEM)] * 8,
        out_specs=pl.BlockSpec(memory_space=pltpu.VMEM),
        scratch_shapes=[
            vmem((HALO + T, whole), BF16),
            vmem((T, whole), BF16),
            vmem((T, inner), BF16),
            vmem((T, width), BF16),
            vmem((inner, width), BF16),
            vmem((S, 8, T), F32),
            vmem((S, 8, T), F32),
            vmem((HEADS, T), F32),
            vmem((HEADS, T), F32),
            vmem((HEADS, T), F32),
            vmem((T, T), F32),
            vmem((T, T), F32),
            vmem((GROUPS, T, 2 * STATE), BF16),
            vmem((T, inner), F32),
            vmem((T, inner), BF16),
            vmem((GROUPS, STATE, gw), F32),
            vmem((GROUPS, STATE, gw), BF16),
            vmem((GROUPS, STATE, gw), BF16),
            vmem((Y - 1, GROUPS, STATE, gw), BF16),
            vmem((Y - 1, GROUPS, STATE, gw), BF16),
            vmem((T, inner), BF16),
            vmem((T, width), F32),
            vmem((T, width), BF16),
            vmem((S * cap, width), BF16),
            vmem((total, width), BF16),
            vmem((R * cap, ff), BF16),
            vmem((S * nx * cap, width), BF16),
            vmem((S * (nx - 1) * cap, width), BF16),
            vmem((S * (nx - 1) * cap, width), BF16),
            vmem((S * cap, width), BF16),
            vmem((width, ff), BF16),
            vmem((width, ff), BF16),
            vmem((ff, width), BF16),
            dma((6,)), dma((3,)),
            dma((S,)), dma((S,)),
            dma(()), dma(()),
            dma((GROUPS,)), dma((GROUPS,)),
            dma((Y - 1, GROUPS)), dma((Y - 1, GROUPS)),
            dma((S,)), dma((S,)),
            dma((S, R)), dma((S, R)),
            dma((S,)), dma((S,)),
            dma((S, nx)), dma((S, nx)),
            dma((S,)), dma((S,)),
        ],
        compiler_params=pltpu.CompilerParams(
            collective_id=0, has_side_effects=True, vmem_limit_bytes=62 * 1024 * 1024
        ),
        cost_estimate=pl.CostEstimate(
            flops=6 * total * width * ff, bytes_accessed=6 * width * ff, transcendentals=total * ff
        ),
    )(*big, *small)


def per_device(
    skip_connection_stream,
    emitted_valve_unscaled,
    channel_source_mapped,
    hidden_source_mapped,
    probe_mapped_values,
    increment_premapped,
    extra_log_fading,
    channel_fading_speed,
    channel_source_kernel,
    hidden_source_kernel,
    probe_kernel_coefficients,
    cluster_scaling_factor,
    emitted_mapping_matrix,
    standardize_scaling,
    standardize_offset,
    chosen_specialist_ids,
    specialist_mixing_shares,
    specialist_gating_matrices,
    raising_matrices,
    lowering_matrices,
):
    S = lax.axis_size("sp")
    R = lax.axis_size("dp")
    T = skip_connection_stream.shape[1]
    assert T == BLK
    cap = -(-(3 * T // S) // 16) * 16
    big = (
        channel_source_mapped[0], hidden_source_mapped[0], probe_mapped_values[0],
        emitted_valve_unscaled[0], skip_connection_stream[0], emitted_mapping_matrix,
        specialist_gating_matrices[0], raising_matrices[0], lowering_matrices[0],
    )
    small = (
        increment_premapped[0].T, extra_log_fading[0].T, channel_fading_speed,
        channel_source_kernel, hidden_source_kernel, probe_kernel_coefficients,
        cluster_scaling_factor[None, :], standardize_scaling[None, :], standardize_offset[None, :],
        chosen_specialist_ids[0].T, specialist_mixing_shares[0],
    )
    return run_layer(S, R, cap, big, small)[None]


def solution(mesh):
    placed = (
        P("dp", "sp", None),
        P("dp", "sp", None),
        P("dp", "sp", None),
        P("dp", "sp", None),
        P("dp", "sp", None),
        P("dp", None, "sp"),
        P("dp", None, "sp"),
        P(),
        P(),
        P(),
        P(),
        P(),
        P(),
        P(),
        P(),
        P("dp", "sp", None),
        P("dp", "sp", None),
        P("sp", None, "dp"),
        P("sp", None, "dp"),
        P("sp", "dp", None),
    )
    return jax.shard_map(
        per_device, mesh=mesh, in_specs=placed, out_specs=P("dp", "sp", None), check_vma=False
    )
```

time: 157 us -> 132 us (0.84)
  Pallas kernels: 104 us -> 128 us
  waiting for transfers between devices: 18.1 us -> 0 us
  starting transfers between devices: 11.2 us -> 0 us
  matrix products: 10.7 us -> 0 us
  other arithmetic: 4.09 us -> 0 us
  local copies, waits for them, and re-layouts: 7.14 us -> 3.29 us
    pallas_call x1, Pallas kernels: 104 us -> 128 us  [run_layer(): pl.pallas_call(functools.partial(layer_kernel, S, R, Y, cap), out_shape=j...]
    all_to_all x2 -> x0, waiting for transfers between devices: 18.1 us -> none  [the longest x1 10.2 us: per_device(): lax.all_to_all(payload.reshape(tok_rows, sp_size * sent_width), 'sp', spl...]
    all_to_all x2 -> x0, starting transfers between devices: 11.2 us -> none  [the longest x1 6.28 us: per_device(): lax.all_to_all(payload.reshape(tok_rows, sp_size * sent_width), 'sp', spl...]
    dot_general x8 -> x0, matrix products: 10.7 us -> none  [the longest x2 3.41 us: per_device(): jnp.dot(picking, answered, preferred_element_type=jnp.float32)]
    unnamed x41 -> x2, local copies, waits for them, and re-layouts: 3.73 us -> 3.29 us
  transfers between devices with their start and end apart: 2 -> 0, of which waited for: 2 -> 0; matrix products, arithmetic and copies ran while one was open for 2% -> 0% of each run, Pallas kernels for 0% -> 0%
where the time goes in v1:
time: 132 us; the launch traced here: 131 us
  Pallas kernels  128 us (97%)
  local copies, waits for them, and re-layouts  3.29 us (2%)
    pallas_call x1, Pallas kernels, run_layer(): pl.pallas_call(functools.partial(layer_kernel, S, R, Y, cap), out_shape=j...  128 us
    unnamed x2, local copies, waits for them, and re-layouts  3.29 us

profile of v1, /device:TPU:8, one launch (start us, length us, event | category | flops | bytes accessed | tf_op | source)
XLA Modules:
  0.0 131.4 jit_solution(174316471064528167)
XLA Ops:
  0.0 1.4 %copy.21 = f32[1,128,2]{2,1,0:T(8,128)} copy(f32[1,128,2]{1,2,0:T(2,128)} %param.36) | data formatting | bytes 2048 | tf_op args[16]
  1.4 128.1 %shard_map.190 = bf16[128,2048]{1,0:T(8,128)(2,1)} custom-call(bf16[128,1024]{1,0:T(8,128)(2,1)} %bitcast.28, bf16[128,256]{1,0:T(8,128)(2,1)} %bitcast.30, bf16[128,256]{1,0:T(8,128)(2,1)} %bitcast.31, bf16[128,1024]{1,0:T(8,128)(2,1)} %bitcast.29, bf16[128,2048]{1,0:T(8,128)(2,1)} %bitcast.27, bf16[1024,2048]{1,0:T(8,128)(2,1)} %wo_hbm.1, ...), custom_call_target="tpu_custom_call" | custom-call | flops 24159191040 | bytes 15728640 | tf_op jit(solution)/shard_map/pallas_call | solution.py:535
  129.6 1.9 %copy.23 = bf16[1,128,2048]{2,1,0:T(8,128)(2,1)} copy(bf16[1,128,2048]{2,1,0:T(8,128)(2,1)} %bitcast.22) | data formatting | bytes 1048576

commit v2 on v1

--- a/solution.py
+++ b/solution.py
@@ -1,4 +1,5 @@
 import functools
+import math
 
 import jax
 import jax.numpy as jnp
@@ -43,6 +44,36 @@
         value = value + jnp.where(lanes >= step, pltpu.roll(value, step, 1), 0.0)
         step *= 2
     return value
+
+
+ISSUE_OF_8 = "5 6 2 3 7 4 1"
+PLAN_OF_8 = """
+A0 A5 A1 R5 A6 G5 D5 A2 R6 C5 G6 A7 A3 R2 D6 R0 G2 D2 R7 C2 G7 F5 R3 C6 R1 D7
+G3 A4 C7 F2 D3 F6 G1 C3 R4 D1 G4 F7 D4 C4 F3 C1 G0 D0 F4 C0 F1 F0
+"""
+
+
+def expert_plan(S):
+    if S == 8:
+        return (
+            [0] + [int(j) for j in ISSUE_OF_8.split()],
+            [(word[0], int(word[1:])) for word in PLAN_OF_8.split()],
+        )
+    order = list(range(S))
+    plan = [("A", j) for j in order[:2]]
+    for p, j in enumerate(order):
+        plan += [("R", j), ("G", j)]
+        if p + 2 < S:
+            plan.append(("A", order[p + 2]))
+        if p > 1:
+            plan.append(("F", order[p - 2]))
+        if p:
+            plan.append(("C", order[p - 1]))
+        plan.append(("D", j))
+    if S > 1:
+        plan.append(("F", order[S - 2]))
+    plan += [("C", order[S - 1]), ("F", order[S - 1])]
+    return order, plan
 
 
 def layer_kernel(
@@ -164,7 +195,8 @@
         relative = jnp.bitwise_xor(ids_ref[k : k + 1, :], s)
         targets.append(relative * cap + rank.astype(I32))
         rows[3 * H + k : 3 * H + k + 1, :] = targets[k].astype(F32)
-    rows[3 * H + 2 :, :] = jnp.zeros((rows.shape[0] - 3 * H - 2, T), F32)
+    rows[3 * H + 2 : 3 * H + 4, :] = share_ref[...]
+    rows[3 * H + 4 :, :] = jnp.zeros((rows.shape[0] - 3 * H - 4, T), F32)
 
     @pl.when(s > 0)
     def _():
@@ -341,8 +373,7 @@
 
     lax.fori_loop(0, T // tile, normalise, 0)
 
-    order = list(range(S))
-    ahead = 2
+    issue, plan = expert_plan(S)
 
     def slot_rows(j, dc, dx, count=1):
         return pl.ds((j * R + dc * nx + dx) * cap, count * cap)
@@ -383,7 +414,7 @@
         else:
             arr[slot_rows(0, 0, 0), :] = moved
 
-    for j in order:
+    for j in issue:
         place(j)
 
     def arrive(j):
@@ -455,31 +486,19 @@
         else:
             ret[pl.ds(0, cap), :] = total.astype(BF16)
 
-    for j in order[:ahead]:
-        arrive(j)
-    weights[0].wait()
-    weights[1].wait()
-    for p, j in enumerate(order):
-        relay(j)
-        gate_up(j)
-        if p + ahead < S:
-            arrive(order[p + ahead])
-        if p == 0:
+    stages = dict(A=arrive, R=relay, G=gate_up, D=down, C=chip_sum, F=finish)
+    for at, (stage, j) in enumerate(plan):
+        if stage == "G" and not any(name == "G" for name, _ in plan[:at]):
+            weights[0].wait()
+            weights[1].wait()
+        if stage == "D" and not any(name == "D" for name, _ in plan[:at]):
             weights[2].wait()
-        if p > 1:
-            finish(order[p - 2])
-        if p:
-            chip_sum(order[p - 1])
-        down(j)
-    if S > 1:
-        finish(order[S - 2])
-    chip_sum(order[S - 1])
-    finish(order[S - 1])
+        stages[stage](j)
 
     target_cols = [cols[:, 3 * H + k : 3 * H + k + 1].astype(I32) for k in range(2)]
-    shares = [share_ref[:, k : k + 1] for k in range(2)]
+    shares = [cols[:, 3 * H + 2 + k : 3 * H + 3 + k] for k in range(2)]
     pre[...] = normed[...].astype(F32)
-    for j in order:
+    for j in [0] + [j for stage, j in plan if stage == "F" and j]:
         if j:
             back(j).wait_recv()
         slot = iota((T, cap), 1) + j * cap
@@ -532,6 +551,43 @@
     vmem = pltpu.VMEM
     total = S * R * cap
     whole = inner + 2 * span
+    buffers = [
+        vmem((HALO + T, whole), BF16),
+        vmem((T, whole), BF16),
+        vmem((T, inner), BF16),
+        vmem((T, width), BF16),
+        vmem((inner, width), BF16),
+        vmem((S, 8, T), F32),
+        vmem((S, 8, T), F32),
+        vmem((HEADS, T), F32),
+        vmem((HEADS, T), F32),
+        vmem((HEADS, T), F32),
+        vmem((T, T), F32),
+        vmem((T, T), F32),
+        vmem((GROUPS, T, 2 * STATE), BF16),
+        vmem((T, inner), F32),
+        vmem((T, inner), BF16),
+        vmem((GROUPS, STATE, gw), F32),
+        vmem((GROUPS, STATE, gw), BF16),
+        vmem((GROUPS, STATE, gw), BF16),
+        vmem((Y - 1, GROUPS, STATE, gw), BF16),
+        vmem((Y - 1, GROUPS, STATE, gw), BF16),
+        vmem((T, inner), BF16),
+        vmem((T, width), F32),
+        vmem((T, width), BF16),
+        vmem((S * cap, width), BF16),
+        vmem((total, width), BF16),
+        vmem((R * cap, ff), BF16),
+        vmem((S * nx * cap, width), BF16),
+        vmem((S * (nx - 1) * cap, width), BF16),
+        vmem((S * (nx - 1) * cap, width), BF16),
+        vmem((S * cap, width), BF16),
+        vmem((width, ff), BF16),
+        vmem((width, ff), BF16),
+        vmem((ff, width), BF16),
+    ]
+    held = sum(b.dtype.itemsize * math.prod(b.shape) for b in buffers)
+    limit = min(62 * 2**20, held + 12 * 2**20)
     return pl.pallas_call(
         functools.partial(layer_kernel, S, R, Y, cap),
         out_shape=jax.ShapeDtypeStruct((T, width), BF16),
@@ -540,40 +596,7 @@
         + [pl.BlockSpec(memory_space=pltpu.SMEM)]
         + [pl.BlockSpec(memory_space=pltpu.VMEM)] * 8,
         out_specs=pl.BlockSpec(memory_space=pltpu.VMEM),
-        scratch_shapes=[
-            vmem((HALO + T, whole), BF16),
-            vmem((T, whole), BF16),
-            vmem((T, inner), BF16),
-            vmem((T, width), BF16),
-            vmem((inner, width), BF16),
-            vmem((S, 8, T), F32),
-            vmem((S, 8, T), F32),
-            vmem((HEADS, T), F32),
-            vmem((HEADS, T), F32),
-            vmem((HEADS, T), F32),
-            vmem((T, T), F32),
-            vmem((T, T), F32),
-            vmem((GROUPS, T, 2 * STATE), BF16),
-            vmem((T, inner), F32),
-            vmem((T, inner), BF16),
-            vmem((GROUPS, STATE, gw), F32),
-            vmem((GROUPS, STATE, gw), BF16),
-            vmem((GROUPS, STATE, gw), BF16),
-            vmem((Y - 1, GROUPS, STATE, gw), BF16),
-            vmem((Y - 1, GROUPS, STATE, gw), BF16),
-            vmem((T, inner), BF16),
-            vmem((T, width), F32),
-            vmem((T, width), BF16),
-            vmem((S * cap, width), BF16),
-            vmem((total, width), BF16),
-            vmem((R * cap, ff), BF16),
-            vmem((S * nx * cap, width), BF16),
-            vmem((S * (nx - 1) * cap, width), BF16),
-            vmem((S * (nx - 1) * cap, width), BF16),
-            vmem((S * cap, width), BF16),
-            vmem((width, ff), BF16),
-            vmem((width, ff), BF16),
-            vmem((ff, width), BF16),
+        scratch_shapes=buffers + [
             dma((6,)), dma((3,)),
             dma((S,)), dma((S,)),
             dma(()), dma(()),
@@ -586,7 +609,7 @@
             dma((S,)), dma((S,)),
         ],
         compiler_params=pltpu.CompilerParams(
-            collective_id=0, has_side_effects=True, vmem_limit_bytes=62 * 1024 * 1024
+            collective_id=0, has_side_effects=True, vmem_limit_bytes=limit
         ),
         cost_estimate=pl.CostEstimate(
             flops=6 * total * width * ff, bytes_accessed=6 * width * ff, transcendentals=total * ff
@@ -630,7 +653,7 @@
         increment_premapped[0].T, extra_log_fading[0].T, channel_fading_speed,
         channel_source_kernel, hidden_source_kernel, probe_kernel_coefficients,
         cluster_scaling_factor[None, :], standardize_scaling[None, :], standardize_offset[None, :],
-        chosen_specialist_ids[0].T, specialist_mixing_shares[0],
+        chosen_specialist_ids[0].T, specialist_mixing_shares[0].T,
     )
     return run_layer(S, R, cap, big, small)[None]
 

time: 132 us -> 123 us (0.932)
  Pallas kernels: 128 us -> 109 us
  local copies, waits for them, and re-layouts: 3.29 us -> 13 us
    pallas_call x1, Pallas kernels: 128 us -> 109 us  [run_layer(): pl.pallas_call(functools.partial(layer_kernel, S, R, Y, cap), out_shape=j...]
    unnamed x2 -> x33, local copies, waits for them, and re-layouts: 3.29 us -> 13 us
where the time goes in v2:
time: 123 us; the launch traced here: 122 us
  Pallas kernels  109 us (89%)
  local copies, waits for them, and re-layouts  13 us (11%)
    pallas_call x1, Pallas kernels, run_layer(): pl.pallas_call(functools.partial(layer_kernel, S, R, Y, cap), out_shape=j...  109 us
    unnamed x33, local copies, waits for them, and re-layouts  13 us

profile of v2, /device:TPU:8, one launch (start us, length us, event | category | flops | bytes accessed | tf_op | source)
XLA Modules:
  0.0 122.5 jit_solution(12468168698864194784)
XLA Ops:
  0.0 0.0 copy-start
  0.0 1.0 copy-done
  1.0 0.9 copy-done.1
  2.0 0.0 copy-start.2
  2.0 0.9 copy-done.2
  2.9 0.0 copy-start.3
  2.9 0.8 copy-done.3
  3.8 0.0 copy-start.4
  3.8 0.8 copy-done.4
  4.6 0.0 copy-start.5
  4.6 0.7 copy-done.5
  5.3 0.0 copy-start.6
  5.3 0.7 copy-done.6
  6.0 0.7 copy-done.7
  6.7 0.7 copy-done.8
  7.4 0.7 copy-done.9
  8.1 0.7 copy-done.10
  8.8 0.7 copy-done.11
  9.5 0.7 copy-done.12
  10.2 0.7 copy-done.13
  10.9 0.7 copy-done.14
  11.6 0.7 copy-done.15
  12.2 109.4 %shard_map.190 = bf16[128,2048]{1,0:T(8,128)(2,1)S(1)} custom-call(bf16[128,1024]{1,0:T(8,128)(2,1)S(1)} %bitcast.26, bf16[128,256]{1,0:T(8,128)(2,1)S(1)} %bitcast.28, bf16[128,256]{1,0:T(8,128)(2,1)S(1)} %bitcast.29, bf16[128,1024]{1,0:T(8,128)(2,1)S(1)} %bitcast.27, bf16[128,2048]{1,0:T(8,128)(2,1)S(1)} %bitcast.25, bf16[1024,2048]{1,0:T(8,128)(2,1)} %wo_hbm.1, ...), custom_call_target="tpu_custom_call" | custom-call | flops 24159191040 | bytes 15728640 | tf_op jit(solution)/shard_map/pallas_call | solution.py:591
  121.7 0.8 copy.22
  (10 shorter events, 0.0 us)
Async XLA Ops:
  0.0 1.0 copy-start
  1.0 0.9 copy-start.1
  2.0 0.9 copy-start.2
  2.9 0.8 copy-start.3
  3.8 0.8 copy-start.4
  4.6 0.7 copy-start.5
  5.3 0.7 copy-start.6
  6.0 0.7 copy-start.7
  6.7 0.7 copy-start.8
  7.4 0.7 copy-start.9
  8.1 0.7 copy-start.10
  8.8 0.7 copy-start.11
  9.5 0.7 copy-start.12
  10.2 0.7 copy-start.13
  10.9 0.7 copy-start.14
  11.6 0.7 copy-start.15

commit v3 on v2

--- a/solution.py
+++ b/solution.py
@@ -1,5 +1,4 @@
 import functools
-import math
 
 import jax
 import jax.numpy as jnp
@@ -18,6 +17,7 @@
 RMS_EPS = 1e-06
 NORM_EPS = 1e-05
 HALO = 16
+PARTS = 1
 MESH = pl.DeviceIdType.MESH
 F32 = jnp.float32
 BF16 = jnp.bfloat16
@@ -46,55 +46,67 @@
     return value
 
 
-ISSUE_OF_8 = "5 6 2 3 7 4 1"
-PLAN_OF_8 = """
-A0 A5 A1 R5 A6 G5 D5 A2 R6 C5 G6 A7 A3 R2 D6 R0 G2 D2 R7 C2 G7 F5 R3 C6 R1 D7
-G3 A4 C7 F2 D3 F6 G1 C3 R4 D1 G4 F7 D4 C4 F3 C1 G0 D0 F4 C0 F1 F0
-"""
+ISSUE_OF_8 = (
+    50, 60, 20, 30, 70, 40, 10,
+)
+PLAN_OF_8 = (
+    0, 50, 10, 150, 60, 250, 350, 20, 160, 450, 260, 70, 30, 120, 360, 100, 220, 320, 170, 420, 270, 550, 130,
+    460, 110, 370, 230, 40, 470, 520, 330, 560, 210, 430, 140, 310, 240, 570, 340, 440, 530, 410, 200, 300,
+    540, 400, 510, 500,
+)
 
 
 def expert_plan(S):
     if S == 8:
         return (
-            [0] + [int(j) for j in ISSUE_OF_8.split()],
-            [(word[0], int(word[1:])) for word in PLAN_OF_8.split()],
+            [(0, h) for h in range(PARTS)] + [divmod(code, 10) for code in ISSUE_OF_8],
+            [(code // 100, code // 10 % 10, code % 10) for code in PLAN_OF_8],
         )
     order = list(range(S))
-    plan = [("A", j) for j in order[:2]]
+    plan = [(0, j) for j in order[:2]]
     for p, j in enumerate(order):
-        plan += [("R", j), ("G", j)]
+        plan += [(1, j), (2, j)]
         if p + 2 < S:
-            plan.append(("A", order[p + 2]))
+            plan.append((0, order[p + 2]))
         if p > 1:
-            plan.append(("F", order[p - 2]))
+            plan.append((5, order[p - 2]))
         if p:
-            plan.append(("C", order[p - 1]))
-        plan.append(("D", j))
+            plan.append((4, order[p - 1]))
+        plan.append((3, j))
     if S > 1:
-        plan.append(("F", order[S - 2]))
-    plan += [("C", order[S - 1]), ("F", order[S - 1])]
-    return order, plan
+        plan.append((5, order[S - 2]))
+    plan += [(4, order[S - 1]), (5, order[S - 1])]
+    return (
+        [(j, h) for j in order for h in range(PARTS)],
+        [(stage, j, h) for stage, j in plan for h in range(1 if stage == 2 else PARTS)],
+    )
 
 
 def layer_kernel(
     S, R, Y, cap,
     xs_hbm, bs_hbm, cs_hbm, valve_hbm, skip_hbm, wo_hbm, wg_hbm, wu_hbm, wd_hbm,
-    inc_ref, fade_ref, speed_ref, xk_ref, bk_ref, ck_ref, gain_ref, lns_ref, lno_ref,
-    ids_ref, share_ref,
-    out_ref,
-    joined, conv, valve, skip, wo, msg, rbuf, step_rows, decay_rows, total_rows, rows, cols,
-    cmask, diag, scaled, state, sendz, recvz, sendy, recvy, normed_g, pre, normed,
-    outb, arr, hid, ra, rx, sx, ret, wg, wu, wd,
-    in_sem, w_sem, m_s, m_r, h_s, h_r, z_s, z_r, y_s, y_r,
-    d_s, d_r, g_s, g_r, a_s, a_r, x_s, x_r, b_s, b_r,
+    *rest,
 ):
+    small_hbm, (out_ref, *rest) = rest[:11], rest[11:]
+    small_vmem, rest = rest[:11], rest[11:]
+    (
+        inc_ref, fade_ref, speed_ref, xk_ref, bk_ref, ck_ref, gain_ref, lns_ref, lno_ref,
+        ids_ref, share_ref,
+    ) = small_vmem
+    (
+        joined, conv, valve, skip, wo, msg, rbuf, step_rows, decay_rows, total_rows, rows, cols,
+        cmask, diag, scaled, state, sendz, recvz, sendy, recvy, normed_g, pre, normed,
+        outb, arr, hid, ra, rx, sx, ret, wg, wu, wd,
+        in_sem, t_sem, w_sem, m_s, m_r, h_s, h_r, z_s, z_r, y_s, y_r,
+        d_s, d_r, g_s, g_r, a_s, a_r, x_s, x_r, b_s, b_r,
+    ) = rest
     s = lax.axis_index("sp")
     d = lax.axis_index("dp")
     T, inner = xs_hbm.shape
     span = bs_hbm.shape[1]
     width = skip_hbm.shape[1]
     ff = wg_hbm.shape[1]
-    hc = inc_ref.shape[0]
+    hc = small_hbm[0].shape[0]
     H = HEADS
     G = GROUPS
     gw = inner // G
@@ -126,7 +138,8 @@
         local(src, dst, w_sem.at[i])
         for i, (src, dst) in enumerate(((wg_hbm, wg), (wu_hbm, wu), (wd_hbm, wd)))
     ]
-    for load in loads:
+    tables = [local(src, dst, t_sem.at[i]) for i, (src, dst) in enumerate(zip(small_hbm, small_vmem))]
+    for load in tables[:3] + loads[:3] + tables[3:] + loads[3:]:
         load.start()
 
     barrier = pltpu.get_barrier_semaphore()
@@ -135,11 +148,15 @@
     for peer in peers:
         pl.semaphore_signal(barrier, inc=1, device_id=peer, device_id_type=MESH)
 
+    for load in tables[:3]:
+        load.wait()
     step_in = jax.nn.softplus(inc_ref[...])
     own_rows = iota((hc, 1), 0)
     speeds = jnp.zeros((hc, 1), F32)
     for i in range(hc):
-        speeds = jnp.where(own_rows == i, speed_ref[s * hc + i], speeds)
+        own = iota((1, H), 1) == s * hc + i
+        speed = jnp.sum(jnp.where(own, speed_ref[...], 0.0), axis=1, keepdims=True)
+        speeds = jnp.where(own_rows == i, speed, speeds)
     decay_in = fade_ref[...] - speeds * step_in
     tot_lanes = iota((hc, T), 1)
     totals_in = jnp.zeros((hc, T), F32)
@@ -183,6 +200,9 @@
     @pl.when(zi == 0)
     def _():
         recvz[...] = jnp.zeros(recvz.shape, BF16)
+
+    for load in tables[3:]:
+        load.wait()
 
     experts = iota((S, T), 0)
     hot = [(ids_ref[k : k + 1, :] == experts) for k in range(2)]
@@ -375,63 +395,76 @@
 
     issue, plan = expert_plan(S)
 
+    half_width = width // PARTS
+
+    def half(h):
+        return pl.ds(h * half_width, half_width)
+
     def slot_rows(j, dc, dx, count=1):
         return pl.ds((j * R + dc * nx + dx) * cap, count * cap)
 
-    def disp(j):
-        return remote(outb.at[pl.ds(j * cap, cap)], arr.at[slot_rows(j, 0, 0)],
-                      d_s.at[j], d_r.at[j], {"sp": flip(s, j)})
-
-    def agx(j, dx):
-        return remote(arr.at[slot_rows(j, 0, 0)], arr.at[slot_rows(j, 0, dx)],
-                      g_s.at[j, dx], g_r.at[j, dx], {"dp": flip(d, 2 * dx)})
-
-    def agc(j, dx):
-        return remote(arr.at[slot_rows(j, 0, dx)], arr.at[slot_rows(j, 1, dx)],
-                      g_s.at[j, nx + dx], g_r.at[j, nx + dx], {"dp": flip(d, 1)})
-
-    def rsc(j):
-        return remote(arr.at[slot_rows(j, 1, 0, nx)], ra.at[pl.ds(j * nx * cap, nx * cap)],
-                      a_s.at[j], a_r.at[j], {"dp": flip(d, 1)})
-
-    def rsx(j, dx):
-        at = pl.ds((j * (nx - 1) + dx - 1) * cap, cap)
-        return remote(sx.at[at], rx.at[at], x_s.at[j, dx], x_r.at[j, dx], {"dp": flip(d, 2 * dx)})
-
-    def back(j):
-        return remote(outb.at[pl.ds(j * cap, cap)], ret.at[pl.ds(j * cap, cap)],
-                      b_s.at[j], b_r.at[j], {"sp": flip(s, j)})
-
-    def place(j):
+    def of(j):
+        return pl.ds(j * cap, cap)
+
+    def beside(j, dx):
+        return pl.ds((j * (nx - 1) + dx - 1) * cap, cap)
+
+    def disp(j, h):
+        return remote(outb.at[of(j), half(h)], arr.at[slot_rows(j, 0, 0), half(h)],
+                      d_s.at[j, h], d_r.at[j, h], {"sp": flip(s, j)})
+
+    def agx(j, dx, h):
+        return remote(arr.at[slot_rows(j, 0, 0), half(h)], arr.at[slot_rows(j, 0, dx), half(h)],
+                      g_s.at[j, dx, h], g_r.at[j, dx, h], {"dp": flip(d, 2 * dx)})
+
+    def agc(j, dx, h):
+        return remote(arr.at[slot_rows(j, 0, dx), half(h)], arr.at[slot_rows(j, 1, dx), half(h)],
+                      g_s.at[j, nx + dx, h], g_r.at[j, nx + dx, h], {"dp": flip(d, 1)})
+
+    def rsc(j, h):
+        return remote(arr.at[slot_rows(j, 1, 0, nx), half(h)],
+                      ra.at[pl.ds(j * nx * cap, nx * cap), half(h)],
+                      a_s.at[j, h], a_r.at[j, h], {"dp": flip(d, 1)})
+
+    def rsx(j, dx, h):
+        return remote(sx.at[beside(j, dx), half(h)], rx.at[beside(j, dx), half(h)],
+                      x_s.at[j, dx, h], x_r.at[j, dx, h], {"dp": flip(d, 2 * dx)})
+
+    def back(j, h):
+        return remote(outb.at[of(j), half(h)], ret.at[of(j), half(h)],
+                      b_s.at[j, h], b_r.at[j, h], {"sp": flip(s, j)})
+
+    def place(j, h):
         slot = iota((cap, T), 0) + j * cap
         hit = jnp.logical_or(slot == targets[0], slot == targets[1])
         moved = jnp.dot(
-            hit.astype(F32).astype(BF16), normed[...], preferred_element_type=F32
+            hit.astype(F32).astype(BF16), normed[:, half(h)], preferred_element_type=F32
         ).astype(BF16)
         if j:
-            outb[pl.ds(j * cap, cap), :] = moved
-            disp(j).start()
+            outb[of(j), half(h)] = moved
+            disp(j, h).start()
         else:
-            arr[slot_rows(0, 0, 0), :] = moved
-
-    for j in issue:
-        place(j)
-
-    def arrive(j):
+            arr[slot_rows(0, 0, 0), half(h)] = moved
+
+    for j, h in issue:
+        place(j, h)
+
+    def arrive(j, h):
         if j:
-            disp(j).wait_recv()
+            disp(j, h).wait_recv()
         for dx in range(1, nx):
-            agx(j, dx).start()
-        agc(j, 0).start()
-
-    def relay(j):
+            agx(j, dx, h).start()
+        agc(j, 0, h).start()
+
+    def relay(j, h):
         for dx in range(1, nx):
-            agx(j, dx).wait_recv()
-            agc(j, dx).start()
-
-    def gate_up(j):
-        for dx in range(nx):
-            agc(j, dx).wait_recv()
+            agx(j, dx, h).wait_recv()
+            agc(j, dx, h).start()
+
+    def gate_up(j, _):
+        for h in range(PARTS):
+            for dx in range(nx):
+                agc(j, dx, h).wait_recv()
         wide = 256 if ff % 256 == 0 else 128
 
         def piece(i, carry):
@@ -444,63 +477,66 @@
 
         lax.fori_loop(0, ff // wide, piece, 0)
 
-    def down(j):
+    def down(j, h):
         for dx in range(nx):
             if dx:
-                agx(j, dx).wait_send()
-            agc(j, dx).wait_send()
-        wide = 256 if width % 256 == 0 else 128
+                agx(j, dx, h).wait_send()
+            agc(j, dx, h).wait_send()
+        wide = 256 if half_width % 256 == 0 else 128
 
         def piece(i, carry):
-            at = pl.ds(pl.multiple_of(i * wide, wide), wide)
+            at = pl.ds(pl.multiple_of(h * half_width + i * wide, wide), wide)
             arr[slot_rows(j, 0, 0, R), at] = jnp.dot(
                 hid[...], wd[:, at], preferred_element_type=F32
             ).astype(BF16)
             return carry
 
-        lax.fori_loop(0, width // wide, piece, 0)
-        rsc(j).start()
-
-    def chip_sum(j):
-        rsc(j).wait_recv()
+        lax.fori_loop(0, half_width // wide, piece, 0)
+        rsc(j, h).start()
+
+    def chip_sum(j, h):
+        rsc(j, h).wait_recv()
         for dx in range(1, nx):
             both = (
-                arr[slot_rows(j, 0, dx), :].astype(F32)
-                + ra[pl.ds((j * nx + dx) * cap, cap), :].astype(F32)
+                arr[slot_rows(j, 0, dx), half(h)].astype(F32)
+                + ra[pl.ds((j * nx + dx) * cap, cap), half(h)].astype(F32)
             )
-            sx[pl.ds((j * (nx - 1) + dx - 1) * cap, cap), :] = both.astype(BF16)
-            rsx(j, dx).start()
-
-    def finish(j):
+            sx[beside(j, dx), half(h)] = both.astype(BF16)
+            rsx(j, dx, h).start()
+
+    def finish(j, h):
         total = (
-            arr[slot_rows(j, 0, 0), :].astype(F32)
-            + ra[pl.ds(j * nx * cap, cap), :].astype(F32)
+            arr[slot_rows(j, 0, 0), half(h)].astype(F32)
+            + ra[pl.ds(j * nx * cap, cap), half(h)].astype(F32)
         )
         for dx in range(1, nx):
-            rsx(j, dx).wait_recv()
-            total = total + rx[pl.ds((j * (nx - 1) + dx - 1) * cap, cap), :].astype(F32)
+            rsx(j, dx, h).wait_recv()
+            total = total + rx[beside(j, dx), half(h)].astype(F32)
         if j:
-            disp(j).wait_send()
-            outb[pl.ds(j * cap, cap), :] = total.astype(BF16)
-            back(j).start()
+            disp(j, h).wait_send()
+            outb[of(j), half(h)] = total.astype(BF16)
+            back(j, h).start()
         else:
-            ret[pl.ds(0, cap), :] = total.astype(BF16)
-
-    stages = dict(A=arrive, R=relay, G=gate_up, D=down, C=chip_sum, F=finish)
-    for at, (stage, j) in enumerate(plan):
-        if stage == "G" and not any(name == "G" for name, _ in plan[:at]):
+            ret[of(0), half(h)] = total.astype(BF16)
+
+    stages = (arrive, relay, gate_up, down, chip_sum, finish)
+    seen = set()
+    for stage, j, h in plan:
+        if stage == 2 and stage not in seen:
             weights[0].wait()
             weights[1].wait()
-        if stage == "D" and not any(name == "D" for name, _ in plan[:at]):
+        if stage == 3 and stage not in seen:
             weights[2].wait()
-        stages[stage](j)
+        seen.add(stage)
+        stages[stage](j, h)
 
     target_cols = [cols[:, 3 * H + k : 3 * H + k + 1].astype(I32) for k in range(2)]
     shares = [cols[:, 3 * H + 2 + k : 3 * H + 3 + k] for k in range(2)]
     pre[...] = normed[...].astype(F32)
-    for j in [0] + [j for stage, j in plan if stage == "F" and j]:
+    ends = [(j, h) for stage, j, h in plan if stage == 5]
+    for j, h in [end for end in ends if end[0] == 0] + [end for end in ends if end[0]]:
         if j:
-            back(j).wait_recv()
+            back(j, h).wait_recv()
         slot = iota((T, cap), 1) + j * cap
         hit = jnp.logical_or(slot == target_cols[0], slot == target_cols[1])
         share = jnp.zeros((T, 1), F32)
@@ -508,9 +544,9 @@
             inside = jnp.logical_and(target_cols[k] >= j * cap, target_cols[k] < (j + 1) * cap)
             share = share + jnp.where(inside, shares[k], 0.0)
         moved = jnp.dot(
-            hit.astype(F32).astype(BF16), ret[pl.ds(j * cap, cap), :], preferred_element_type=F32
-        )
-        pre[...] = pre[...] + share * moved
+            hit.astype(F32).astype(BF16), ret[of(j), half(h)], preferred_element_type=F32
+        )
+        pre[:, half(h)] = pre[:, half(h)] + share * moved
     out_ref[...] = pre[...].astype(BF16)
 
     for j in range(1, S):
@@ -528,12 +564,13 @@
     for g in range(G):
         for dy in range(1, Y):
             along_y(dy, g).wait_send()
-    for j in range(S):
-        rsc(j).wait_send()
-        for dx in range(1, nx):
-            rsx(j, dx).wait_send()
-        if j:
-            back(j).wait_send()
+    for h in range(PARTS):
+        for j in range(S):
+            rsc(j, h).wait_send()
+            for dx in range(1, nx):
+                rsx(j, dx, h).wait_send()
+            if j:
+                back(j, h).wait_send()
 
 
 def run_layer(S, R, cap, big, small):
@@ -551,7 +588,7 @@
     vmem = pltpu.VMEM
     total = S * R * cap
     whole = inner + 2 * span
-    buffers = [
+    buffers = [vmem(table.shape, table.dtype) for table in small] + [
         vmem((HALO + T, whole), BF16),
         vmem((T, whole), BF16),
         vmem((T, inner), BF16),
@@ -586,30 +623,25 @@
         vmem((width, ff), BF16),
         vmem((ff, width), BF16),
     ]
-    held = sum(b.dtype.itemsize * math.prod(b.shape) for b in buffers)
-    limit = min(62 * 2**20, held + 12 * 2**20)
     return pl.pallas_call(
         functools.partial(layer_kernel, S, R, Y, cap),
         out_shape=jax.ShapeDtypeStruct((T, width), BF16),
-        in_specs=[pl.BlockSpec(memory_space=pl.ANY)] * 9
-        + [pl.BlockSpec(memory_space=pltpu.VMEM)] * 2
-        + [pl.BlockSpec(memory_space=pltpu.SMEM)]
-        + [pl.BlockSpec(memory_space=pltpu.VMEM)] * 8,
+        in_specs=[pl.BlockSpec(memory_space=pl.ANY)] * 20,
         out_specs=pl.BlockSpec(memory_space=pltpu.VMEM),
         scratch_shapes=buffers + [
-            dma((6,)), dma((3,)),
+            dma((6,)), dma((11,)), dma((3,)),
             dma((S,)), dma((S,)),
             dma(()), dma(()),
             dma((GROUPS,)), dma((GROUPS,)),
             dma((Y - 1, GROUPS)), dma((Y - 1, GROUPS)),
-            dma((S,)), dma((S,)),
-            dma((S, R)), dma((S, R)),
-            dma((S,)), dma((S,)),
-            dma((S, nx)), dma((S, nx)),
-            dma((S,)), dma((S,)),
+            dma((S, PARTS)), dma((S, PARTS)),
+            dma((S, R, PARTS)), dma((S, R, PARTS)),
+            dma((S, PARTS)), dma((S, PARTS)),
+            dma((S, nx, PARTS)), dma((S, nx, PARTS)),
+            dma((S, PARTS)), dma((S, PARTS)),
         ],
         compiler_params=pltpu.CompilerParams(
-            collective_id=0, has_side_effects=True, vmem_limit_bytes=limit
+            collective_id=0, has_side_effects=True, vmem_limit_bytes=62 * 2**20
         ),
         cost_estimate=pl.CostEstimate(
             flops=6 * total * width * ff, bytes_accessed=6 * width * ff, transcendentals=total * ff
@@ -650,7 +682,7 @@
         specialist_gating_matrices[0], raising_matrices[0], lowering_matrices[0],
     )
     small = (
-        increment_premapped[0].T, extra_log_fading[0].T, channel_fading_speed,
+        increment_premapped[0].T, extra_log_fading[0].T, channel_fading_speed[None, :],
         channel_source_kernel, hidden_source_kernel, probe_kernel_coefficients,
         cluster_scaling_factor[None, :], standardize_scaling[None, :], standardize_offset[None, :],
         chosen_specialist_ids[0].T, specialist_mixing_shares[0].T,

time: 123 us -> 112 us (0.911)
  local copies, waits for them, and re-layouts: 13 us -> 1.88 us
    unnamed x33 -> x1, local copies, waits for them, and re-layouts: 13 us -> 1.88 us
where the time goes in v3:
time: 112 us
  Pallas kernels  110 us (98%)
  local copies, waits for them, and re-layouts  1.88 us (2%)
    pallas_call x1, Pallas kernels, run_layer(): pl.pallas_call(functools.partial(layer_kernel, S, R, Y, cap), out_shape=j...  110 us

profile of v3, /device:TPU:8, one launch (start us, length us, event | category | flops | bytes accessed | tf_op | source)
XLA Modules:
  0.0 111.7 jit_solution(18337688608746772724)
XLA Ops:
  0.0 109.8 %shard_map.190 = bf16[128,2048]{1,0:T(8,128)(2,1)} custom-call(bf16[128,1024]{1,0:T(8,128)(2,1)} %bitcast.30, bf16[128,256]{1,0:T(8,128)(2,1)} %bitcast.32, bf16[128,256]{1,0:T(8,128)(2,1)} %bitcast.33, bf16[128,1024]{1,0:T(8,128)(2,1)} %bitcast.31, bf16[128,2048]{1,0:T(8,128)(2,1)} %bitcast.29, bf16[1024,2048]{1,0:T(8,128)(2,1)} %wo_hbm.1, ...), custom_call_target="tpu_custom_call" | custom-call | flops 24159191040 | bytes 15728640 | tf_op jit(solution)/shard_map/pallas_call | solution.py:626
  109.8 1.9 %copy.22 = bf16[1,128,2048]{2,1,0:T(8,128)(2,1)} copy(bf16[1,128,2048]{2,1,0:T(8,128)(2,1)} %bitcast.25) | data formatting | bytes 1048576
